TPU v7x, 32 devices: a whole 2x2x4 slice. The times are simulated.
32 devices in a mesh: fs: 16 (over z, y, x), tp: 2 (over core).
Axes of the slice: x: 2, y: 2, z: 4, core: 2. Of those that a mesh axis runs over, the one named last changes fastest.
Arguments:
- tokens: bfloat16 [4096, 2048], P('fs'), may hold values from -6 to 6
- mix_gain: float32 [2048], replicated, may hold values from 0.1 to 1.9
- glu_value: bfloat16 [2048, 2048], P('fs', 'tp'), may hold values from -0.125 to 0.125
- glu_gate: bfloat16 [2048, 2048], P('fs', 'tp'), may hold values from -0.125 to 0.125
- conv_taps: float32 [31, 2048], P(None, 'tp'), may hold values from -2.2 to 2.2, as said below
- chan_gain: float32 [2048], P('tp'), may hold values from 0.1 to 1.9
- mix_out: bfloat16 [2048, 2048], P('tp', 'fs'), may hold values from -0.125 to 0.125
- mlp_gain: float32 [2048], replicated, may hold values from 0.1 to 1.9
- up_weight: bfloat16 [2048, 8192], P('fs', 'tp'), may hold values from -0.125 to 0.125
- down_weight: bfloat16 [8192, 2048], P('tp', 'fs'), may hold values from -0.0625 to 0.0625
Outputs:
- result: bfloat16 [4096, 2048], P('fs')
Inputs may be any that keep to these rules, and one draw needn't show every extreme that they name: `conv_taps`: independent entries scaled by fan-in; channels fall into 16 groups of different scale.
All inputs are finite; a program needn't handle non-finite values.
Results may differ from a plain program's by a relative error of at most 0.018.
Values may be sent and summed in bfloat16 or wider, within the bound.
A program may use at most 128 MiB of HBM per device.

v0:
```python
import jax
import jax.numpy as jnp
from jax import lax
from jax.sharding import PartitionSpec as P

C = 2048
LEN = 128


norm_floor = 0.05


def rms_scale(stream, gain):
    return stream * lax.rsqrt(jnp.mean(stream * stream, axis=-1, keepdims=True) + norm_floor) * gain


def bf16_round(value):
    return lax.optimization_barrier(value.astype(jnp.bfloat16)).astype(jnp.float32)


def depthwise(glu, conv_taps):
    seqs = glu.shape[0] // LEN
    blocks = glu.reshape(seqs, LEN, glu.shape[1]).astype(jnp.float32)
    reach = conv_taps.shape[0] // 2
    padded = jnp.pad(blocks, ((0, 0), (reach, reach), (0, 0)))
    total = jnp.zeros_like(blocks)
    for offset in range(conv_taps.shape[0]):
        total = total + padded[:, offset : offset + LEN] * conv_taps[offset]
    return total.reshape(glu.shape)


def per_device(
    tokens,
    mix_gain,
    glu_value,
    glu_gate,
    conv_taps,
    chan_gain,
    mix_out,
    mlp_gain,
    up_weight,
    down_weight,
):
    stream = tokens.astype(jnp.float32)
    normed = rms_scale(stream, mix_gain).astype(jnp.bfloat16)
    values = jnp.dot(
        normed,
        lax.all_gather(glu_value, "fs", axis=0, tiled=True),
        preferred_element_type=jnp.float32,
    )
    gating = jnp.dot(
        normed,
        lax.all_gather(glu_gate, "fs", axis=0, tiled=True),
        preferred_element_type=jnp.float32,
    )
    glu = (values * jax.nn.sigmoid(gating)).astype(jnp.bfloat16)
    convolved = depthwise(glu, conv_taps)
    sums, squares = lax.psum(
        (jnp.sum(convolved, axis=-1), jnp.sum(convolved * convolved, axis=-1)), "tp"
    )
    centre = (sums / C)[:, None]
    spread = (squares / C)[:, None] - centre * centre
    hidden = jax.nn.silu((convolved - centre) * lax.rsqrt(spread + norm_floor) * chan_gain).astype(
        jnp.bfloat16
    )
    whole_out = lax.all_gather(mix_out, "fs", axis=1, tiled=True)
    own_rows = stream.shape[0] // lax.axis_size("tp")
    mixed = lax.psum_scatter(
        jnp.dot(hidden, whole_out, preferred_element_type=jnp.float32).astype(jnp.bfloat16),
        "tp",
        scatter_dimension=0,
        tiled=True,
    ).astype(jnp.float32)
    own_stream = lax.dynamic_slice_in_dim(stream, lax.axis_index("tp") * own_rows, own_rows, 0)
    resid = own_stream + bf16_round(mixed)
    normed_mlp = rms_scale(resid, mlp_gain).astype(jnp.bfloat16)
    whole_up = lax.all_gather(up_weight, "fs", axis=0, tiled=True)
    active = jnp.square(
        jax.nn.relu(
            jnp.dot(
                lax.all_gather(normed_mlp, "tp", axis=0, tiled=True),
                whole_up,
                preferred_element_type=jnp.float32,
            )
        )
    ).astype(jnp.bfloat16)
    whole_down = lax.all_gather(down_weight, "fs", axis=1, tiled=True)
    feed = lax.psum_scatter(
        jnp.dot(active, whole_down, preferred_element_type=jnp.float32).astype(jnp.bfloat16),
        "tp",
        scatter_dimension=0,
        tiled=True,
    ).astype(jnp.float32)
    finished = (resid + bf16_round(feed)).astype(jnp.bfloat16)
    return lax.all_gather(finished, "tp", axis=0, tiled=True)


def solution(mesh):
    in_specs = (
        P("fs", None),
        P(),
        P("fs", "tp"),
        P("fs", "tp"),
        P(None, "tp"),
        P("tp"),
        P("tp", "fs"),
        P(),
        P("fs", "tp"),
        P("tp", "fs"),
    )
    out_specs = P("fs", None)
    return jax.shard_map(
        per_device, mesh=mesh, in_specs=in_specs, out_specs=out_specs, check_vma=False
    )
```

profile of v0, /device:TPU:0, one launch (start us, length us, event | category | flops | bytes accessed | tf_op | source)
XLA Modules:
  0.0 769.7 jit_solution(15755725362399529471)
XLA Ops:
  6.5 0.7 all-gather.10.cloned.1.call-update
  7.3 0.7 all-gather.8.cloned.1.call-update
  8.1 0.7 all-gather.12.cloned.1.call-update
  8.8 1.5 multiply_reduce_fusion
  10.3 1.1 fusion.72
  11.4 1.4 fusion.71
  12.9 75.6 %all-gather.10.cloned.1.call-done = bf16[2048,1024]{1,0:T(8,128)(2,1)} async-done(((bf16[128,1024]{1,0:T(8,128)(2,1)}), bf16[2048,1024]{1,0:T(8,128)(2,1)}) %all-gather.10.cloned.1.call-update) | async-done | bytes 4194320 | tf_op jit(solution)/shard_map/all_gather | solution.py:53
  88.4 3.9 fusion.4
  92.4 73.1 %all-gather.8.cloned.1.call-done = bf16[2048,1024]{1,0:T(8,128)(2,1)} async-done(((bf16[128,1024]{1,0:T(8,128)(2,1)}), bf16[2048,1024]{1,0:T(8,128)(2,1)}) %all-gather.8.cloned.1.call-update) | async-done | bytes 4194320 | tf_op jit(solution)/shard_map/all_gather | solution.py:48
  165.4 3.5 bitcast_convert_fusion
  169.0 5.7 fusion.69
  174.7 2.5 all-reduce.1
  177.2 0.4 multiply_convert_fusion.2
  177.6 77.9 %all-gather.12.cloned.1.call-done = bf16[1024,2048]{1,0:T(8,128)(2,1)} async-done(((bf16[1024,128]{1,0:T(8,128)(2,1)}), bf16[1024,2048]{1,0:T(8,128)(2,1)}) %all-gather.12.cloned.1.call-update) | async-done | bytes 4194320 | tf_op jit(solution)/shard_map/all_gather | solution.py:66
  255.5 4.4 convolution_convert_fusion.1
  259.9 0.0 all-gather.14.cloned.1.call-start
  260.0 0.2 convert_element_type.45
  260.2 6.4 reduce-scatter.3.cloned.1.call-done
  266.7 1.3 multiply_reduce_fusion.1
  267.9 2.0 multiply_convert_fusion.1
  270.0 0.0 all-gather.16.cloned.1.call-start
  270.0 0.5 all-gather.16.cloned.1.call-update
  270.6 0.7 all-gather.18.cloned.1.call-update
  271.4 9.0 %all-gather.14.cloned.1.call-done = bf16[256,2048]{1,0:T(8,128)(2,1)} async-done(((bf16[128,2048]{1,0:T(8,128)(2,1)}), bf16[256,2048]{1,0:T(8,128)(2,1)}) %all-gather.14.cloned.1.call-update) | async-done | bytes 1048592 | tf_op jit(solution)/shard_map/all_gather | solution.py:81
  280.4 194.8 %all-gather.16.cloned.1.call-done = bf16[2048,4096]{1,0:T(8,128)(2,1)} async-done(((bf16[128,4096]{1,0:T(8,128)(2,1)}), bf16[2048,4096]{1,0:T(8,128)(2,1)}) %all-gather.16.cloned.1.call-update) | async-done | bytes 16777232 | tf_op jit(solution)/shard_map/all_gather | solution.py:77
  475.2 250.0 %all-gather.18.cloned.1.call-done = bf16[4096,2048]{1,0:T(8,128)(2,1)} async-done(((bf16[4096,128]{1,0:T(8,128)(2,1)}), bf16[4096,2048]{1,0:T(8,128)(2,1)}) %all-gather.18.cloned.1.call-update) | async-done | bytes 16777232 | tf_op jit(solution)/shard_map/all_gather | solution.py:87
  725.2 16.4 %convolution_convert_fusion = bf16[256,2048]{1,0:T(8,128)(2,1)} fusion(bf16[4096,2048]{1,0:T(8,128)(2,1)} %all-gather.18.cloned.1.call-done, bf16[256,2048]{1,0:T(8,128)(2,1)} %all-gather.14.cloned.1.call-done, bf16[2048,4096]{1,0:T(8,128)(2,1)} %all-gather.16.cloned.1.call-done), kind=kOutput, calls=%fused_computation.33 | convolution fusion | flops 8593604608 | bytes 35651584 | tf_op jit(solution)/shard_map/dot_general | solution.py:89
  741.7 0.0 all-gather.20.cloned.1.call-start
  741.8 6.7 reduce-scatter.5.cloned.1.call-done
  748.4 2.0 add_convert_fusion
  750.5 10.4 %all-gather.20.cloned.1.call-done = bf16[256,2048]{1,0:T(8,128)(2,1)} async-done(((bf16[128,2048]{1,0:T(8,128)(2,1)}), bf16[256,2048]{1,0:T(8,128)(2,1)}) %all-gather.20.cloned.1.call-update) | async-done | bytes 1048592 | tf_op jit(solution)/shard_map/all_gather | solution.py:95
  760.9 2.3 copy.12
  (23 shorter events, 0.3 us)
Async XLA Ops:
  6.5 81.9 %all-gather.10.cloned.1.call-start = ((), (), s32[]{:S(2)}) async-start(), calls=%async_computation.3 | async-start | bytes 4456448 | tf_op jit(solution)/shard_map/all_gather | solution.py:53
  7.3 158.2 %all-gather.8.cloned.1.call-start = ((), (), s32[]{:S(2)}) async-start(), calls=%async_computation.2 | async-start | bytes 4456448 | tf_op jit(solution)/shard_map/all_gather | solution.py:48
  8.0 247.5 %all-gather.12.cloned.1.call-start = ((), (), s32[]{:S(2)}) async-start(), calls=%async_computation.4 | async-start | bytes 4456448 | tf_op jit(solution)/shard_map/all_gather | solution.py:66
  8.7 257.9 %reduce-scatter.3.cloned.1.call-start = ((), (), s32[]{:S(2)}) async-start(), calls=%async_computation.5 | async-start | bytes 1572864 | tf_op jit(solution)/shard_map/reduce_scatter | solution.py:68
  12.8 152.6 %copy-start.1 = (bf16[256,2048]{1,0:T(8,128)(2,1)S(1)}, bf16[256,2048]{1,0:T(8,128)(2,1)}, u32[]{:S(2)}) copy-start(bf16[256,2048]{1,0:T(8,128)(2,1)} %param.10) | copy-start | bytes 3145732
  12.8 152.6 %copy-start.4 = (f32[2048]{0:T(1024)S(1)}, f32[2048]{0:T(1024)}, u32[]{:S(2)}) copy-start(f32[2048]{0:T(1024)} %param.11) | copy-start | bytes 24580
  92.4 84.8 %copy-start.3 = (f32[1024]{0:T(1024)S(1)}, f32[1024]{0:T(1024)}, u32[]{:S(2)}) copy-start(f32[1024]{0:T(1024)} %param.15) | copy-start | bytes 12292
  259.9 8.0 %copy-start.2 = (f32[2048]{0:T(1024)S(1)}, f32[2048]{0:T(1024)}, u32[]{:S(2)}) copy-start(f32[2048]{0:T(1024)} %param.17) | copy-start | bytes 24580
  259.9 20.4 %all-gather.14.cloned.1.call-start = ((), (), s32[]{:S(2)}) async-start(), calls=%async_computation.6 | async-start | bytes 1572864 | tf_op jit(solution)/shard_map/all_gather | solution.py:81
  270.0 205.2 %all-gather.16.cloned.1.call-start = ((), (), s32[]{:S(2)}) async-start(), calls=%async_computation.7 | async-start | bytes 17825792 | tf_op jit(solution)/shard_map/all_gather | solution.py:77
  270.6 454.7 %all-gather.18.cloned.1.call-start = ((), (), s32[]{:S(2)}) async-start(), calls=%async_computation.8 | async-start | bytes 17825792 | tf_op jit(solution)/shard_map/all_gather | solution.py:87
  271.3 477.1 %copy-start = (bf16[128,2048]{1,0:T(8,128)(2,1)S(1)}, bf16[128,2048]{1,0:T(8,128)(2,1)}, u32[]{:S(2)}) copy-start(bf16[128,2048]{1,0:T(8,128)(2,1)} %reduce-scatter.3.cloned.1.call-done) | copy-start | bytes 1572868
  271.3 477.1 %reduce-scatter.5.cloned.1.call-start = ((), (), s32[]{:S(2)}) async-start(), calls=%async_computation.9 | async-start | bytes 1572864 | tf_op jit(solution)/shard_map/reduce_scatter | solution.py:88
  741.7 19.2 %all-gather.20.cloned.1.call-start = ((), (), s32[]{:S(2)}) async-start(), calls=%async_computation.10 | async-start | bytes 1572864 | tf_op jit(solution)/shard_map/all_gather | solution.py:95
Sparse Core Ops, SparseCore 0:
  10.1 78.3 all-gather.9
  91.2 74.1 all-gather.7
  168.1 87.3 all-gather.11
  260.1 6.5 reduce-scatter.2
  270.1 10.2 all-gather.13
  283.0 192.1 all-gather.15
  477.9 247.2 all-gather.17
  741.8 6.5 reduce-scatter.4
  750.6 10.2 all-gather.19
where the time goes:
time: 770 us
  waiting for transfers between devices  707 us (92%)
  matrix products  28.3 us (4%)
  between operations  13.3 us (2%)
  other arithmetic  13.2 us (2%)
    all_gather x1, waiting for transfers between devices, per_device(): whole_down = lax.all_gather(down_weight, 'fs', axis=1, tiled=True)  250 us
    all_gather x1, waiting for transfers between devices, per_device(): whole_up = lax.all_gather(up_weight, 'fs', axis=0, tiled=True)  195 us
    all_gather x1, waiting for transfers between devices, per_device(): whole_out = lax.all_gather(mix_out, 'fs', axis=1, tiled=True)  77.9 us
    all_gather x1, waiting for transfers between devices, per_device(): lax.all_gather(glu_gate, 'fs', axis=0, tiled=True)  75.6 us
    all_gather x1, waiting for transfers between devices, per_device(): lax.all_gather(glu_value, 'fs', axis=0, tiled=True)  73.1 us
    dot_general x1, matrix products, per_device(): jnp.dot(active, whole_down, preferred_element_type=jnp.float32)  16.4 us
  transfers between devices with their start and end apart: 9, of which 9 were waited for; matrix products, arithmetic and copies ran while one was open for 2% of the time, Pallas kernels for 0%

commit v1 on v0

v1 whole, which is shorter than its diff:
```python
import jax
import jax.numpy as jnp
from jax import lax
from jax.sharding import PartitionSpec as P

C = 2048
LEN = 128


norm_floor = 0.05


def rms_scale(stream, gain):
    return stream * lax.rsqrt(jnp.mean(stream * stream, axis=-1, keepdims=True) + norm_floor) * gain


def bf16_round(value):
    return lax.optimization_barrier(value.astype(jnp.bfloat16)).astype(jnp.float32)


def depthwise(glu, conv_taps):
    seqs = glu.shape[0] // LEN
    blocks = glu.reshape(seqs, LEN, glu.shape[1]).astype(jnp.float32)
    reach = conv_taps.shape[0] // 2
    padded = jnp.pad(blocks, ((0, 0), (reach, reach), (0, 0)))
    total = jnp.zeros_like(blocks)
    for offset in range(conv_taps.shape[0]):
        total = total + padded[:, offset : offset + LEN] * conv_taps[offset]
    return total.reshape(glu.shape)


def swap_then_gather(weight, inner, outer, split, join):
    own = lax.all_to_all(
        weight, "fs", split_axis=split, concat_axis=join, axis_index_groups=inner, tiled=True
    )
    return lax.all_gather(own, "fs", axis=join, axis_index_groups=outer, tiled=True)


def shared_sum(partial, inner, tp):
    part = lax.all_to_all(
        partial, "fs", split_axis=0, concat_axis=0, axis_index_groups=inner, tiled=True
    )
    group = len(inner[0])
    rows = partial.shape[0] // group
    part = part.reshape(group, tp, rows // tp, -1).transpose(1, 0, 2, 3)
    part = lax.all_to_all(part, "tp", split_axis=0, concat_axis=0, tiled=True)
    return bf16_round(jnp.sum(part.astype(jnp.float32), axis=(0, 1)))


def per_device(
    tokens,
    mix_gain,
    glu_value,
    glu_gate,
    conv_taps,
    chan_gain,
    mix_out,
    mlp_gain,
    up_weight,
    down_weight,
):
    fs, tp = lax.axis_size("fs"), lax.axis_size("tp")
    group = 4 if fs % 4 == 0 else 1
    inner = [[o * group + i for i in range(group)] for o in range(fs // group)]
    outer = [[o * group + i for o in range(fs // group)] for i in range(group)]
    place = lax.rem(lax.axis_index("fs"), group)

    value_w = swap_then_gather(glu_value, inner, outer, 1, 0)
    gate_w = swap_then_gather(glu_gate, inner, outer, 1, 0)
    mix_w = swap_then_gather(mix_out, inner, outer, 0, 1)
    up_w = swap_then_gather(up_weight, inner, outer, 1, 0)
    down_w = swap_then_gather(down_weight, inner, outer, 0, 1)

    stream = tokens.astype(jnp.float32)
    normed = rms_scale(stream, mix_gain).astype(jnp.bfloat16)
    normed = lax.all_gather(normed, "fs", axis=0, axis_index_groups=inner, tiled=True)
    values = jnp.dot(normed, value_w, preferred_element_type=jnp.float32)
    gating = jnp.dot(normed, gate_w, preferred_element_type=jnp.float32)
    glu = (values * jax.nn.sigmoid(gating)).astype(jnp.bfloat16)
    channels = value_w.shape[1]
    taps = lax.dynamic_slice_in_dim(conv_taps, place * channels, channels, 1)
    gain = lax.dynamic_slice_in_dim(chan_gain, place * channels, channels, 0)
    convolved = depthwise(glu, taps)
    both = jnp.stack(
        (jnp.sum(convolved, axis=-1), jnp.sum(convolved * convolved, axis=-1))
    )
    both = jnp.sum(lax.all_gather(both, "fs", axis=0, axis_index_groups=inner), axis=0)
    both = lax.psum(both, "tp")
    centre = (both[0] / C)[:, None]
    spread = (both[1] / C)[:, None] - centre * centre
    hidden = jax.nn.silu((convolved - centre) * lax.rsqrt(spread + norm_floor) * gain).astype(
        jnp.bfloat16
    )
    mixed = shared_sum(
        jnp.dot(hidden, mix_w, preferred_element_type=jnp.float32).astype(jnp.bfloat16), inner, tp
    )
    own_rows = stream.shape[0] // tp
    own_stream = lax.dynamic_slice_in_dim(stream, lax.axis_index("tp") * own_rows, own_rows, 0)
    resid = own_stream + mixed
    normed_mlp = rms_scale(resid, mlp_gain).astype(jnp.bfloat16)
    normed_mlp = lax.all_gather(normed_mlp, "fs", axis=0, axis_index_groups=inner)
    normed_mlp = lax.all_gather(normed_mlp, "tp", axis=1).reshape(-1, normed.shape[1])
    active = jnp.square(
        jax.nn.relu(jnp.dot(normed_mlp, up_w, preferred_element_type=jnp.float32))
    ).astype(jnp.bfloat16)
    feed = shared_sum(
        jnp.dot(active, down_w, preferred_element_type=jnp.float32).astype(jnp.bfloat16), inner, tp
    )
    finished = (resid + feed).astype(jnp.bfloat16)
    return lax.all_gather(finished, "tp", axis=0, tiled=True)

def solution(mesh):
    in_specs = (
        P("fs", None),
        P(),
        P("fs", "tp"),
        P("fs", "tp"),
        P(None, "tp"),
        P("tp"),
        P("tp", "fs"),
        P(),
        P("fs", "tp"),
        P("tp", "fs"),
    )
    out_specs = P("fs", None)
    return jax.shard_map(
        per_device, mesh=mesh, in_specs=in_specs, out_specs=out_specs, check_vma=False
    )
```

time: 770 us -> 559 us (0.73)
  waiting for transfers between devices: 707 us -> 326 us
  blocking collectives: 2.47 us -> 147 us
  local copies, waits for them, and re-layouts: 4.85 us -> 19.1 us
  starting transfers between devices: 0.32 us -> 8.9 us
    all_gather x6 -> x8, waiting for transfers between devices: 680 us -> 267 us  [the longest x5 199 us: swap_then_gather(): lax.all_gather(own, 'fs', axis=join, axis_index_groups=outer, tiled=True)]
    all_to_all x0 -> x7, blocking collectives: none -> 136 us  [the longest x4 67.7 us: swap_then_gather(): lax.all_to_all(weight, 'fs', split_axis=split, concat_axis=join, axis_ind...]
    all_to_all x0 -> x2, waiting for transfers between devices: none -> 49.1 us  [the longest x1 46.9 us: shared_sum(): lax.all_to_all(partial, 'fs', split_axis=0, concat_axis=0, axis_index_gro...]
    reduce_scatter x2 -> x0, waiting for transfers between devices: 13.1 us -> none  [the longest x1 6.68 us: per_device(): lax.psum_scatter(jnp.dot(active, whole_down, preferred_element_type=jnp.f...]
    all_to_all x0 -> x2, starting transfers between devices: none -> 8.39 us  [the longest x1 4.97 us: shared_sum(): lax.all_to_all(partial, 'fs', split_axis=0, concat_axis=0, axis_index_gro...]
    all_gather x0 -> x1, blocking collectives: none -> 8.15 us  [per_device(): lax.all_gather(both, 'fs', axis=0, axis_index_groups=inner)]
  transfers between devices with their start and end apart: 9 -> 11, of which waited for: 9 -> 10; matrix products, arithmetic and copies ran while one was open for 2% -> 5% of each run, Pallas kernels for 0% -> 0%
where the time goes in v1:
time: 559 us; the launch traced here: 558 us
  waiting for transfers between devices  326 us (58%)
  blocking collectives  147 us (26%)
  matrix products  26.3 us (5%)
  local copies, waits for them, and re-layouts  19.1 us (3%)
  other arithmetic  17.4 us (3%)
  between operations  13.4 us (2%)
  starting transfers between devices  8.9 us (2%)
    all_gather x5, waiting for transfers between devices, swap_then_gather(): lax.all_gather(own, 'fs', axis=join, axis_index_groups=outer, tiled=True)  199 us
    all_to_all x4, blocking collectives, swap_then_gather(): lax.all_to_all(weight, 'fs', split_axis=split, concat_axis=join, axis_ind...  67.7 us
    all_gather x1, waiting for transfers between devices, per_device(): lax.all_gather(normed, 'fs', axis=0, axis_index_groups=inner, tiled=True)  53.8 us
    all_to_all x1, blocking collectives, shared_sum(): lax.all_to_all(partial, 'fs', split_axis=0, concat_axis=0, axis_index_gro...  52.3 us
    all_to_all x1, waiting for transfers between devices, shared_sum(): lax.all_to_all(partial, 'fs', split_axis=0, concat_axis=0, axis_index_gro...  46.9 us
    all_to_all x2, blocking collectives, shared_sum(): part = lax.all_to_all(part, 'tp', split_axis=0, concat_axis=0, tiled=True)  16.3 us
    dot_general x1, matrix products, per_device(): jnp.dot(active, down_w, preferred_element_type=jnp.float32)  14.4 us
    all_gather x1, waiting for transfers between devices, per_device(): lax.all_gather(normed_mlp, 'tp', axis=1).reshape(-1, normed.shape[1])  13.7 us
  transfers between devices with their start and end apart: 11, of which 10 were waited for; matrix products, arithmetic and copies ran while one was open for 5% of the time, Pallas kernels for 0%

profile of v1, /device:TPU:0, one launch (start us, length us, event | category | flops | bytes accessed | tf_op | source)
XLA Modules:
  0.0 557.7 jit_solution(16136352445515227430)
XLA Ops:
  7.7 10.7 %all_to_all.123 = bf16[128,4,256]{0,2,1:T(8,128)(2,1)S(1)} all-to-all(bf16[128,4,256]{0,2,1:T(8,128)(2,1)S(1)} %bitcast.102), channel_id=1, replica_groups={{0,2,4,6},{8,10,12,14},{16,18,20,22},{24,26,28,30},{1,3,5,7},{9,11,13,1..., dimensions={1} | all-to-all | bytes 524288 | tf_op jit(solution)/shard_map/all_to_all | solution.py:33
  20.9 2.5 multiply_convert_fusion.1
  23.6 8.1 %all_to_all.124 = bf16[128,4,256]{0,2,1:T(8,128)(2,1)S(1)} all-to-all(bf16[128,4,256]{0,2,1:T(8,128)(2,1)S(1)} %bitcast.103), channel_id=1, replica_groups={{0,2,4,6},{8,10,12,14},{16,18,20,22},{24,26,28,30},{1,3,5,7},{9,11,13,1..., dimensions={1} | all-to-all | bytes 524288 | tf_op jit(solution)/shard_map/all_to_all | solution.py:33
  32.7 3.4 all-to-all-start.2
  42.3 4.9 all-gather.18.cloned.1.call-done
  47.2 53.8 %all-gather.14.cloned.1.call-done = bf16[1024,2048]{1,0:T(8,128)(2,1)} async-done(((bf16[256,2048]{1,0:T(8,128)(2,1)}), bf16[1024,2048]{1,0:T(8,128)(2,1)}) %all-gather.14.cloned.1.call-update) | async-done | bytes 4194320 | tf_op jit(solution)/shard_map/all_gather | solution.py:76
  101.0 3.8 fusion.2
  104.7 25.8 %all-gather.16.cloned.1.call-done = bf16[2048,256]{1,0:T(8,128)(2,1)} async-done(((bf16[512,256]{1,0:T(8,128)(2,1)}), bf16[2048,256]{1,0:T(8,128)(2,1)}) %all-gather.16.cloned.1.call-update) | async-done | bytes 1048592 | tf_op jit(solution)/shard_map/all_gather | solution.py:36
  130.6 3.7 bitcast_convert_fusion
  134.3 4.5 fusion.67
  138.8 8.2 %all-gather.3 = f32[4,2,1024]{2,1,0:T(2,128)S(1)} all-gather(f32[1,2,1024]{2,1,0:T(2,128)S(1)} %maximum_bitcast_fusion), channel_id=2, replica_groups={{0,2,4,6},{8,10,12,14},{16,18,20,22},{24,26,28,30},{1,3,5,7},{9,11,13,1..., dimensions={0}, use_global_device_ids=true | all-gather | bytes 40960 | tf_op jit(solution)/shard_map/all_gather | solution.py:87
  147.0 2.5 psum.7
  149.9 9.4 %all-gather.20.cloned.1.call-done = bf16[256,2048]{0,1:T(8,128)(2,1)} async-done(((bf16[256,512]{0,1:T(8,128)(2,1)}), bf16[256,2048]{0,1:T(8,128)(2,1)}) %all-gather.20.cloned.1.call-update) | async-done | bytes 1048592 | tf_op jit(solution)/shard_map/all_gather | solution.py:36
  159.4 4.5 convolution_convert_fusion
  163.8 5.0 all-to-all-start.3
  169.1 46.9 %all-to-all-done.3 = bf16[4,256,2048]{2,1,0:T(8,128)(2,1)} async-done(((bf16[4,256,2048]{2,1,0:T(8,128)(2,1)}), bf16[4,256,2048]{2,1,0:T(8,128)(2,1)}, u32[]{:S(2)}, u32[]{:S(2)}) %all-to-all-start.3) | async-done | bytes 4194336 | tf_op jit(solution)/shard_map/all_to_all | solution.py:40
  216.0 2.5 copy.32
  218.5 8.2 %all_to_all.125 = bf16[2,4,128,2048]{3,2,1,0:T(8,128)(2,1)} all-to-all(bf16[2,4,128,2048]{3,2,1,0:T(8,128)(2,1)S(1)} %copy.32), channel_id=1, replica_groups=mesh['fs'=16,'tp'=2] {'tp'}, dimensions={0} | all-to-all | bytes 8388608 | tf_op jit(solution)/shard_map/all_to_all | solution.py:46
  226.7 3.0 reduce_sum.73
  231.0 24.7 %all_to_all.126 = bf16[4,1024,128]{2,1,0:T(8,128)(2,1)} all-to-all(bf16[4,1024,128]{2,1,0:T(8,128)(2,1)} %bitcast.95), channel_id=1, replica_groups={{0,2,4,6},{8,10,12,14},{16,18,20,22},{24,26,28,30},{1,3,5,7},{9,11,13,1..., dimensions={0} | all-to-all | bytes 2097152 | tf_op jit(solution)/shard_map/all_to_all | solution.py:33
  258.0 2.3 copy.33
  260.3 24.2 %all_to_all.127 = bf16[128,4,1024]{0,2,1:T(8,128)(2,1)} all-to-all(bf16[128,4,1024]{0,2,1:T(8,128)(2,1)} %bitcast.93), channel_id=1, replica_groups={{0,2,4,6},{8,10,12,14},{16,18,20,22},{24,26,28,30},{1,3,5,7},{9,11,13,1..., dimensions={1} | all-to-all | bytes 2097152 | tf_op jit(solution)/shard_map/all_to_all | solution.py:33
  284.5 2.3 copy.34
  287.8 78.2 %all-gather.24.cloned.1.call-done = bf16[1024,2048]{0,1:T(8,128)(2,1)} async-done(((bf16[1024,512]{0,1:T(8,128)(2,1)}), bf16[1024,2048]{0,1:T(8,128)(2,1)}) %all-gather.24.cloned.1.call-update) | async-done | bytes 4194320 | tf_op jit(solution)/shard_map/all_gather | solution.py:36
  366.0 80.8 %all-gather.22.cloned.1.call-done = bf16[2048,1024]{1,0:T(8,128)(2,1)} async-done(((bf16[512,1024]{1,0:T(8,128)(2,1)}), bf16[2048,1024]{1,0:T(8,128)(2,1)}) %all-gather.22.cloned.1.call-update) | async-done | bytes 4194320 | tf_op jit(solution)/shard_map/all_gather | solution.py:36
  446.8 13.7 %all-gather.30.cloned.1.call-done = bf16[4,256,2048]{2,1,0:T(8,128)(2,1)} async-done(((bf16[4,128,2048]{2,1,0:T(8,128)(2,1)}), bf16[4,256,2048]{2,1,0:T(8,128)(2,1)}) %all-gather.30.cloned.1.call-update) | async-done | bytes 4194320 | tf_op jit(solution)/shard_map/all_gather | solution.py:102
  460.5 14.4 %convolution_convert_fusion.1 = bf16[1024,2048]{1,0:T(8,128)(2,1)} fusion(bf16[1024,2048]{0,1:T(8,128)(2,1)} %all-gather.24.cloned.1.call-done, bf16[1024,2048]{1,0:T(8,128)(2,1)} %bitcast.140, bf16[2048,1024]{1,0:T(8,128)(2,1)} %all-gather.22.cloned.1.call-done), kind=kOutput, calls=%fused_computation.2 | convolution fusion | flops 8595177472 | bytes 16777216 | tf_op jit(solution)/shard_map/dot_general | solution.py:107
  474.9 52.3 %all_to_all.128 = bf16[4,256,2048]{2,1,0:T(8,128)(2,1)S(1)} all-to-all(bf16[4,256,2048]{2,1,0:T(8,128)(2,1)} %bitcast.88), channel_id=1, replica_groups={{0,2,4,6},{8,10,12,14},{16,18,20,22},{24,26,28,30},{1,3,5,7},{9,11,13,1..., dimensions={0} | all-to-all | bytes 8388608 | tf_op jit(solution)/shard_map/all_to_all | solution.py:40
  527.8 8.2 %all_to_all.129 = bf16[2,4,128,2048]{3,2,1,0:T(8,128)(2,1)} all-to-all(bf16[2,4,128,2048]{3,2,1,0:T(8,128)(2,1)S(1)} %copy.36), channel_id=1, replica_groups=mesh['fs'=16,'tp'=2] {'tp'}, dimensions={0} | all-to-all | bytes 8388608 | tf_op jit(solution)/shard_map/all_to_all | solution.py:46
  536.0 3.0 reduce_sum.75
  539.9 8.9 %all-gather.26.cloned.1.call-done = bf16[256,2048]{1,0:T(8,128)(2,1)} async-done(((bf16[128,2048]{1,0:T(8,128)(2,1)}), bf16[256,2048]{1,0:T(8,128)(2,1)}) %all-gather.26.cloned.1.call-update) | async-done | bytes 1048592 | tf_op jit(solution)/shard_map/all_gather | solution.py:110
  548.8 2.3 copy.38
  (48 shorter events, 17.7 us)
Async XLA Ops:
  6.5 16.9 %copy-start.1 = (bf16[128,1024]{1,0:T(8,128)(2,1)S(1)}, bf16[128,1024]{1,0:T(8,128)(2,1)}, u32[]{:S(2)}) copy-start(bf16[128,1024]{1,0:T(8,128)(2,1)} %param.12) | copy-start | bytes 786436
  6.5 40.6 %all-gather.18.cloned.1.call-start = ((), (), s32[]{:S(2)}) async-start(), calls=%async_computation.11 | async-start | bytes 1310720 | tf_op jit(solution)/shard_map/all_gather | solution.py:36
  19.3 81.7 %all-gather.14.cloned.1.call-start = ((), (), s32[]{:S(2)}) async-start(), calls=%async_computation.9 | async-start | bytes 5242880 | tf_op jit(solution)/shard_map/all_gather | solution.py:76
  23.4 107.1 %all-gather.16.cloned.1.call-start = ((), (), s32[]{:S(2)}) async-start(), calls=%async_computation.10 | async-start | bytes 1310720 | tf_op jit(solution)/shard_map/all_gather | solution.py:36
  32.7 8.8 %all-to-all-start.2 = ((bf16[4,256,128]{2,1,0:T(8,128)(2,1)}), bf16[4,256,128]{2,1,0:T(8,128)(2,1)S(1)}, u32[]{:S(2)}, u32[]{:S(2)}) async-start(bf16[4,256,128]{2,1,0:T(8,128)(2,1)} %bitcast.45), calls=%async_computation.2 | async-start | bytes 524288 | tf_op jit(solution)/shard_map/all_to_all | solution.py:33
  36.1 123.3 %all-gather.20.cloned.1.call-start = ((), (), s32[]{:S(2)}) async-start(), calls=%async_computation.12 | async-start | bytes 1310720 | tf_op jit(solution)/shard_map/all_gather | solution.py:36
  163.8 5.0 copy-start
  163.8 52.2 %all-to-all-start.3 = ((bf16[4,256,2048]{2,1,0:T(8,128)(2,1)}), bf16[4,256,2048]{2,1,0:T(8,128)(2,1)}, u32[]{:S(2)}, u32[]{:S(2)}) async-start(bf16[4,256,2048]{2,1,0:T(8,128)(2,1)} %bitcast.86), calls=%async_computation.3 | async-start | bytes 8388608 | tf_op jit(solution)/shard_map/all_to_all | solution.py:40
  168.8 118.0 %all-gather.28.cloned.1.call-start = ((), (), s32[]{:S(2)}) async-start(), calls=%async_computation.16 | async-start | bytes 2621440 | tf_op jit(solution)/shard_map/all_gather | solution.py:101
  226.7 3.2 copy-start.2
  230.9 135.0 %all-gather.24.cloned.1.call-start = ((), (), s32[]{:S(2)}) async-start(), calls=%async_computation.14 | async-start | bytes 5242880 | tf_op jit(solution)/shard_map/all_gather | solution.py:36
  257.9 188.9 %all-gather.22.cloned.1.call-start = ((), (), s32[]{:S(2)}) async-start(), calls=%async_computation.13 | async-start | bytes 5242880 | tf_op jit(solution)/shard_map/all_gather | solution.py:36
  286.8 173.7 %all-gather.30.cloned.1.call-start = ((), (), s32[]{:S(2)}) async-start(), calls=%async_computation.17 | async-start | bytes 6291456 | tf_op jit(solution)/shard_map/all_gather | solution.py:102
  287.6 261.3 %all-gather.26.cloned.1.call-start = ((), (), s32[]{:S(2)}) async-start(), calls=%async_computation.15 | async-start | bytes 1572864 | tf_op jit(solution)/shard_map/all_gather | solution.py:110
Sparse Core Ops, SparseCore 0:
  19.4 27.6 all-gather.17
  49.0 51.9 all-gather.13
  102.5 27.9 all-gather.15
  132.0 27.3 all-gather.19
  231.0 52.0 all-gather.27
  284.5 81.3 all-gather.23
  367.5 79.2 all-gather.21
  448.3 12.1 all-gather.29
  540.1 8.7 all-gather.25

commit v2 on v1

--- a/solution.py
+++ b/solution.py
@@ -1,6 +1,10 @@
+import functools
+
 import jax
 import jax.numpy as jnp
 from jax import lax
+from jax.experimental import pallas as pl
+from jax.experimental.pallas import tpu as pltpu
 from jax.sharding import PartitionSpec as P
 
 C = 2048
@@ -47,7 +51,7 @@
     return bf16_round(jnp.sum(part.astype(jnp.float32), axis=(0, 1)))
 
 
-def per_device(
+def plain_device(
     tokens,
     mix_gain,
     glu_value,
@@ -109,6 +113,385 @@
     finished = (resid + feed).astype(jnp.bfloat16)
     return lax.all_gather(finished, "tp", axis=0, tiled=True)
 
+MESH = pl.DeviceIdType.MESH
+F32, BF16 = jnp.float32, jnp.bfloat16
+
+
+def rows_at(start, size):
+    return pl.ds(pl.multiple_of(start, 128), size)
+
+
+def layer_kernel(
+    ng, nz,
+    tok, mixg, gv, gg, taps, chg, mo, mlpg, up, dn,
+    out,
+    fgv, fgg, fmo, fup, fdn,
+    tok_all, nrm, pad, cv, hid, st, st_all,
+    acc, resid, nm_all, act, fin,
+    sbo1, sbi1, rdo1, rdi1, sbo2, sbi2, rdo2, rdi2,
+    ws, wr, lsem, tsem, nsem, ssem, rsem, fsem,
+):
+    f, t = lax.axis_index("fs"), lax.axis_index("tp")
+    p, z = lax.rem(f, ng), lax.div(f, ng)
+    sib = 1 - t
+    L = tok.shape[0] // 2
+    half = ng * L
+    width = tok.shape[1]
+    chans = fgv.shape[1]
+    hidden = fup.shape[1]
+    depth = gv.shape[0]
+    sends = []
+
+    def chip(dq):
+        return lax.rem(p + dq, ng)
+
+    def plane(dz):
+        return lax.rem(z + dz, nz)
+
+    def push(src, dst, s_sem, r_sem, device):
+        copy = pltpu.make_async_remote_copy(
+            src_ref=src, dst_ref=dst, send_sem=s_sem, recv_sem=r_sem,
+            device_id=device, device_id_type=MESH,
+        )
+        copy.start()
+        sends.append(copy)
+
+    def arrived(dst, s_sem, r_sem):
+        pltpu.make_async_remote_copy(
+            src_ref=dst, dst_ref=dst, send_sem=s_sem, recv_sem=r_sem,
+            device_id=(f, sib), device_id_type=MESH,
+        ).wait_recv()
+
+    barrier = pltpu.get_barrier_semaphore()
+    peers = [(z * ng + chip(dq), u) for dq in range(1, ng) for u in (t, sib)]
+    peers += [(f, sib)] + [(plane(dz) * ng + p, t) for dz in range(1, nz)]
+    for peer in peers:
+        pl.semaphore_signal(barrier, inc=1, device_id=peer, device_id_type=MESH)
+    pl.semaphore_wait(barrier, len(peers))
+
+    weights = (
+        (lambda q: gv.at[:, rows_at(q * chans, chans)], lambda g: fgv.at[rows_at(g * depth, depth), :]),
+        (lambda q: gg.at[:, rows_at(q * chans, chans)], lambda g: fgg.at[rows_at(g * depth, depth), :]),
+        (lambda q: mo.at[rows_at(q * chans, chans), :], lambda g: fmo.at[:, rows_at(g * depth, depth)]),
+        (lambda q: up.at[:, rows_at(q * hidden, hidden)], lambda g: fup.at[rows_at(g * depth, depth), :]),
+        (lambda q: dn.at[rows_at(q * hidden, hidden), :], lambda g: fdn.at[:, rows_at(g * depth, depth)]),
+    )
+
+    def spread_in_plane(a):
+        src, dst = weights[a]
+        for dq in range(1, ng):
+            push(src(chip(dq)), dst(f), ws.at[a, dq], wr.at[a, ng - dq], (z * ng + chip(dq), t))
+
+    def spread_own(a):
+        src, dst = weights[a]
+        for dz in range(1, nz):
+            push(src(p), dst(f), ws.at[a, dz * ng], wr.at[a, (nz - dz) * ng], (plane(dz) * ng + p, t))
+
+    def forward(a):
+        dst = weights[a][1]
+        for dq in range(1, ng):
+            piece = dst(z * ng + chip(dq))
+            arrived(piece, ws.at[a, 0], wr.at[a, dq])
+            for dz in range(1, nz):
+                push(piece, piece, ws.at[a, dz * ng + dq], wr.at[a, (nz - dz) * ng + dq], (plane(dz) * ng + p, t))
+
+    def whole(a):
+        src, dst = weights[a]
+        for dz in range(1, nz):
+            for dq in range(ng):
+                arrived(dst(plane(dz) * ng + chip(dq)), ws.at[a, 0], wr.at[a, dz * ng + dq])
+        local(a).wait()
+
+    def local(a):
+        src, dst = weights[a]
+        return pltpu.make_async_copy(src(p), dst(f), lsem.at[a])
+
+    for a in (0, 1):
+        spread_in_plane(a)
+    for a in (0, 1):
+        spread_own(a)
+    for dq in range(1, ng):
+        push(
+            tok.at[rows_at(t * L, L)], tok_all.at[rows_at(t * half + p * L, L)],
+            tsem.at[0, dq], tsem.at[1, ng - dq], (z * ng + chip(dq), t),
+        )
+    spread_in_plane(2)
+    spread_own(2)
+    for a in (3, 4):
+        spread_in_plane(a)
+    for a in range(5):
+        local(a).start()
+
+    step = 16
+
+    def norm_rows(load, gain, dst, start):
+        def body(i, _):
+            value = load(i * step).astype(F32)
+            scale = lax.rsqrt(jnp.mean(value * value, axis=-1, keepdims=True) + norm_floor)
+            dst[pl.ds(pl.multiple_of(start + i * step, step), step), :] = (
+                value * scale * gain[...]
+            ).astype(BF16)
+            return 0
+
+        lax.fori_loop(0, L // step, body, 0)
+
+    def from_ref(ref, base):
+        return lambda i: ref[pl.ds(pl.multiple_of(base + i, step), step), :]
+
+    for u in range(2):
+        norm_rows(from_ref(tok, u * L), mixg, nrm, u * half + p * L)
+    for a in (0, 1):
+        forward(a)
+    for dq in range(1, ng):
+        block = tok_all.at[rows_at(t * half + chip(dq) * L, L)]
+        arrived(block, tsem.at[0, 0], tsem.at[1, dq])
+        push(block, block, tsem.at[2, dq], tsem.at[3, dq], (f, sib))
+        norm_rows(from_ref(tok_all, t * half + chip(dq) * L), mixg, nrm, t * half + chip(dq) * L)
+    forward(2)
+    for a in (3, 4):
+        spread_own(a)
+    for dq in range(1, ng):
+        start = sib * half + chip(dq) * L
+        arrived(tok_all.at[rows_at(start, L)], tsem.at[0, 0], tsem.at[3, dq])
+        norm_rows(from_ref(tok_all, start), mixg, nrm, start)
+
+    whole(0)
+    whole(1)
+    pad[...] = jnp.zeros_like(pad)
+    st[...] = jnp.zeros_like(st)
+    taps_n = taps.shape[0]
+    reach = taps_n // 2
+    lead = (reach + 7) // 8 * 8
+    own_cols = p * chans
+    eye = lax.broadcasted_iota(jnp.int32, (L, L), 0) == lax.broadcasted_iota(jnp.int32, (L, L), 1)
+
+    def conv_block(b, _):
+        rows = rows_at(b * L, L)
+        left = nrm[rows, :]
+        values = jnp.dot(left, fgv[...], preferred_element_type=F32)
+        gating = jnp.dot(left, fgg[...], preferred_element_type=F32)
+        glu = (values * jax.nn.sigmoid(gating)).astype(BF16).astype(F32)
+        pad[pl.ds(lead, L), :] = glu
+        sums = jnp.zeros((L, 1), F32)
+        squares = jnp.zeros((L, 1), F32)
+        for c in range(chans // 128):
+            total = jnp.zeros((L, 128), F32)
+            for j in range(taps_n):
+                tap = taps[pl.ds(j, 1), rows_at(own_cols + c * 128, 128)]
+                total = total + pad[pl.ds(lead - reach + j, L), pl.ds(c * 128, 128)] * tap
+            cv[rows, pl.ds(c * 128, 128)] = total
+            sums = sums + jnp.sum(total, axis=1, keepdims=True)
+            squares = squares + jnp.sum(total * total, axis=1, keepdims=True)
+        st[b, pl.ds(0, 1), :] = jnp.sum(jnp.where(eye, sums, 0.0), axis=0, keepdims=True)
+        st[b, pl.ds(1, 1), :] = jnp.sum(jnp.where(eye, squares, 0.0), axis=0, keepdims=True)
+        return 0
+
+    lax.fori_loop(0, 2 * ng, conv_block, 0)
+
+    slots = [(dq, du) for dq in range(ng) for du in range(2) if (dq, du) != (0, 0)]
+    for dq, du in slots:
+        push(
+            st, st_all.at[(ng - dq) % ng * 2 + du],
+            ssem.at[0, dq * 2 + du], ssem.at[1, (ng - dq) % ng * 2 + du],
+            (z * ng + chip(dq), t if du == 0 else sib),
+        )
+    forward(3)
+    for dq, du in slots:
+        arrived(st_all.at[dq * 2 + du], ssem.at[0, 0], ssem.at[1, dq * 2 + du])
+
+    def hidden_block(b, _):
+        rows = rows_at(b * L, L)
+        total = st[b]
+        for dq, du in slots:
+            total = total + st_all[dq * 2 + du, b]
+        count = chans * ng * 2
+        sums = jnp.sum(jnp.where(eye, total[0:1, :], 0.0), axis=1, keepdims=True)
+        squares = jnp.sum(jnp.where(eye, total[1:2, :], 0.0), axis=1, keepdims=True)
+        centre = sums / count
+        spread = squares / count - centre * centre
+        value = (cv[rows, :] - centre) * lax.rsqrt(spread + norm_floor)
+        value = value * chg[:, rows_at(own_cols, chans)]
+        hid[rows, :] = (value * jax.nn.sigmoid(value)).astype(BF16)
+        return 0
+
+    lax.fori_loop(0, 2 * ng, hidden_block, 0)
+
+    cols = 512
+
+    def reduce_rows(left, right, sbo, sbi, rdo, rdi, k):
+        def theirs(n, _):
+            at = rows_at(n * cols, cols)
+            sbo[:, at] = jnp.dot(
+                left[rows_at(sib * half, half), :], right[:, at], preferred_element_type=F32
+            ).astype(BF16)
+            return 0
+
+        lax.fori_loop(0, width // cols, theirs, 0)
+        push(sbo, sbi, rsem.at[k, 0], rsem.at[k, 1], (f, sib))
+
+        def mine(n, _):
+            at = rows_at(n * cols, cols)
+            acc[:, at] = jnp.dot(
+                left[rows_at(t * half, half), :], right[:, at], preferred_element_type=F32
+            )
+            return 0
+
+        lax.fori_loop(0, width // cols, mine, 0)
+        arrived(sbi, rsem.at[k, 0], rsem.at[k, 1])
+        for dq in range(1, ng):
+            base = chip(dq) * L
+
+            def add(i, _):
+                at = pl.ds(pl.multiple_of(base + i * step, step), step)
+                rdo[at, :] = (acc[at, :] + sbi[at, :].astype(F32)).astype(BF16)
+                return 0
+
+            lax.fori_loop(0, L // step, add, 0)
+            push(
+                rdo.at[rows_at(base, L)], rdi.at[ng - dq - 1],
+                rsem.at[k, 2 * dq], rsem.at[k, 2 * (ng - dq) + 1], (z * ng + chip(dq), t),
+            )
+
+    def reduced(sbi, rdi, i):
+        at = pl.ds(pl.multiple_of(p * L + i * step, step), step)
+        total = acc[at, :] + sbi[at, :].astype(F32)
+        for dq in range(1, ng):
+            total = total + rdi[dq - 1, pl.ds(pl.multiple_of(i * step, step), step), :].astype(F32)
+        return total.astype(BF16).astype(F32)
+
+    def wait_reduced(rdi, k):
+        for dq in range(1, ng):
+            arrived(rdi.at[dq - 1], rsem.at[k, 0], rsem.at[k, 2 * dq + 1])
+
+    whole(2)
+    reduce_rows(hid, fmo, sbo1, sbi1, rdo1, rdi1, 0)
+    forward(4)
+    wait_reduced(rdi1, 0)
+
+    def resid_rows(i, _):
+        at = pl.ds(pl.multiple_of(i * step, step), step)
+        own = tok[pl.ds(pl.multiple_of(t * L + i * step, step), step), :].astype(F32)
+        value = own + reduced(sbi1, rdi1, i)
+        resid[at, :] = value
+        scale = lax.rsqrt(jnp.mean(value * value, axis=-1, keepdims=True) + norm_floor)
+        nm_all[pl.ds(pl.multiple_of(t * half + p * L + i * step, step), step), :] = (
+            value * scale * mlpg[...]
+        ).astype(BF16)
+        return 0
+
+    lax.fori_loop(0, L // step, resid_rows, 0)
+    mine = nm_all.at[rows_at(t * half + p * L, L)]
+    for dq in range(1, ng):
+        push(mine, mine, nsem.at[0, dq], nsem.at[1, ng - dq], (z * ng + chip(dq), t))
+    push(mine, mine, nsem.at[2, 0], nsem.at[3, 0], (f, sib))
+    for dq in range(1, ng):
+        block = nm_all.at[rows_at(t * half + chip(dq) * L, L)]
+        arrived(block, nsem.at[0, 0], nsem.at[1, dq])
+        push(block, block, nsem.at[2, dq], nsem.at[3, dq], (f, sib))
+
+    whole(3)
+
+    def up_half(u):
+        def body(n, _):
+            at = rows_at(n * 256, 256)
+            value = jnp.dot(
+                nm_all[rows_at(u * half, half), :], fup[:, at], preferred_element_type=F32
+            )
+            value = jnp.maximum(value, 0.0)
+            act[rows_at(u * half, half), at] = (value * value).astype(BF16)
+            return 0
+
+        lax.fori_loop(0, hidden // 256, body, 0)
+
+    up_half(t)
+    for dq in range(ng):
+        arrived(nm_all.at[rows_at(sib * half + chip(dq) * L, L)], nsem.at[0, 0], nsem.at[3, dq])
+    up_half(sib)
+    whole(4)
+    reduce_rows(act, fdn, sbo2, sbi2, rdo2, rdi2, 1)
+    wait_reduced(rdi2, 1)
+
+    def finish_rows(i, _):
+        at = pl.ds(pl.multiple_of(i * step, step), step)
+        value = (resid[at, :] + reduced(sbi2, rdi2, i)).astype(BF16)
+        fin[0, at, :] = value
+        out[pl.ds(pl.multiple_of(t * L + i * step, step), step), :] = value
+        return 0
+
+    lax.fori_loop(0, L // step, finish_rows, 0)
+    push(fin.at[0], fin.at[1], fsem.at[0], fsem.at[1], (f, sib))
+    arrived(fin.at[1], fsem.at[0], fsem.at[1])
+
+    def copy_rows(i, _):
+        at = pl.ds(pl.multiple_of(i * step, step), step)
+        out[pl.ds(pl.multiple_of(sib * L + i * step, step), step), :] = fin[1, at, :]
+        return 0
+
+    lax.fori_loop(0, L // step, copy_rows, 0)
+    for copy in sends:
+        copy.wait_send()
+
+
+def fused_device(ng, nz, tokens, mix_gain, glu_value, glu_gate, conv_taps, chan_gain, mix_out, mlp_gain, up_weight, down_weight):
+    rows, width = tokens.shape
+    fs = ng * nz
+    L = rows // 2
+    half = ng * L
+    chans = glu_value.shape[1] // ng
+    hidden = up_weight.shape[1] // ng
+    depth = glu_value.shape[0]
+    blocks = 2 * ng
+    vm = pltpu.VMEM
+    dma = pltpu.SemaphoreType.DMA
+    reduce_bufs = [
+        vm((half, width), BF16), vm((half, width), BF16), vm((half, width), BF16),
+        vm((ng - 1, L, width), BF16),
+    ]
+    scratch = [
+        vm((fs * depth, chans), BF16), vm((fs * depth, chans), BF16), vm((chans, width), BF16),
+        vm((fs * depth, hidden), BF16), vm((hidden, width), BF16),
+        vm((2 * half, width), BF16), vm((2 * half, width), BF16),
+        vm((L + 32, chans), F32), vm((2 * half, chans), F32), vm((2 * half, chans), BF16),
+        vm((blocks, 8, L), F32), vm((blocks, blocks, 8, L), F32),
+        vm((half, width), F32), vm((L, width), F32), vm((2 * half, width), BF16),
+        vm((2 * half, hidden), BF16), vm((2, L, width), BF16),
+        *reduce_bufs, *reduce_bufs,
+        dma((5, fs)), dma((5, fs)), dma((5,)), dma((4, ng)), dma((4, ng)),
+        dma((2, blocks)), dma((2, 2 * ng)), dma((2,)),
+    ]
+    return pl.pallas_call(
+        functools.partial(layer_kernel, ng, nz),
+        out_shape=jax.ShapeDtypeStruct((rows, width), BF16),
+        in_specs=[pl.BlockSpec(memory_space=vm)] * 10,
+        out_specs=pl.BlockSpec(memory_space=vm),
+        scratch_shapes=scratch,
+        compiler_params=pltpu.CompilerParams(
+            collective_id=0, has_side_effects=True, vmem_limit_bytes=60 * 1024 * 1024
+        ),
+    )(
+        tokens, mix_gain[None], glu_value, glu_gate, conv_taps, chan_gain[None], mix_out,
+        mlp_gain[None], up_weight, down_weight,
+    )
+
+
+def per_device(*args):
+    tokens, glu_value, conv_taps = args[0], args[2], args[4]
+    fs, tp = lax.axis_size("fs"), lax.axis_size("tp")
+    group = 4
+    fits = (
+        tp == 2
+        and fs % group == 0
+        and fs > group
+        and tokens.shape[0] == 2 * LEN
+        and glu_value.shape[0] % 128 == 0
+        and conv_taps.shape[1] % (group * 128) == 0
+        and conv_taps.shape[0] <= 31
+    )
+    if fits:
+        return fused_device(group, fs // group, *args)
+    return plain_device(*args)
+
+
 def solution(mesh):
     in_specs = (
         P("fs", None),

time: 559 us -> 293 us (0.52)
  waiting for transfers between devices: 326 us -> 0 us
  Pallas kernels: 0 us -> 287 us
  blocking collectives: 147 us -> 0 us
  matrix products: 26.3 us -> 0 us
  other arithmetic: 17.4 us -> 0 us
  local copies, waits for them, and re-layouts: 19.1 us -> 2.3 us
  between operations: 13.4 us -> 0.01 us
  starting transfers between devices: 8.9 us -> 0 us
    pallas_call x0 -> x1, Pallas kernels: none -> 287 us  [fused_device(): pl.pallas_call(functools.partial(layer_kernel, ng, nz), out_shape=jax.Sha...]
    all_gather x9 -> x0, waiting for transfers between devices: 276 us -> none  [the longest x5 199 us: swap_then_gather(): lax.all_gather(own, 'fs', axis=join, axis_index_groups=outer, tiled=True)]
    all_to_all x7 -> x0, blocking collectives: 136 us -> none  [the longest x4 67.7 us: swap_then_gather(): lax.all_to_all(weight, 'fs', split_axis=split, concat_axis=join, axis_ind...]
    all_to_all x2 -> x0, waiting for transfers between devices: 49.1 us -> none  [the longest x1 46.9 us: shared_sum(): lax.all_to_all(partial, 'fs', split_axis=0, concat_axis=0, axis_index_gro...]
    dot_general x4 -> x0, matrix products: 26.3 us -> none  [the longest x1 14.4 us: per_device(): jnp.dot(active, down_w, preferred_element_type=jnp.float32)]
    reduce_sum x6 -> x0, other arithmetic: 12.2 us -> none  [the longest x2 5.92 us: shared_sum(): return bf16_round(jnp.sum(part.astype(jnp.float32), axis=(0, 1)))]
    all_to_all x2 -> x0, starting transfers between devices: 8.39 us -> none  [the longest x1 4.97 us: shared_sum(): lax.all_to_all(partial, 'fs', split_axis=0, concat_axis=0, axis_index_gro...]
    all_gather x1 -> x0, blocking collectives: 8.15 us -> none  [per_device(): lax.all_gather(both, 'fs', axis=0, axis_index_groups=inner)]
  transfers between devices with their start and end apart: 11 -> 0, of which waited for: 10 -> 0; matrix products, arithmetic and copies ran while one was open for 5% -> 0% of each run, Pallas kernels for 0% -> 0%
where the time goes in v2:
time: 293 us; the launch traced here: 290 us
  Pallas kernels  287 us (98%)
    pallas_call x1, Pallas kernels, fused_device(): pl.pallas_call(functools.partial(layer_kernel, ng, nz), out_shape=jax.Sha...  287 us

profile of v2, /device:TPU:0, one launch (start us, length us, event | category | flops | bytes accessed | tf_op | source)
XLA Modules:
  0.0 289.8 jit_solution(6049393761033599023)
XLA Ops:
  0.0 287.5 %shard_map.100 = bf16[256,2048]{1,0:T(8,128)(2,1)} custom-call(bf16[256,2048]{1,0:T(8,128)(2,1)} %tok.1, f32[1,2048]{1,0:T(1,128)} %bitcast.3, bf16[128,1024]{1,0:T(8,128)(2,1)} %gv.1, bf16[128,1024]{1,0:T(8,128)(2,1)} %gg.1, f32[31,1024]{1,0:T(8,128)} %taps.1, f32[1,1024]{1,0:T(1,128)} %bitcast.5, bf16[1024,128]{1,0:T(8,128)(2,1)} %mo.1, ...), custom_call_target="tpu_custom_call" | custom-call | tf_op jit(solution)/shard_map/pallas_call | solution.py:462
  287.5 2.3 copy.12

commit v3 on v2

--- a/solution.py
+++ b/solution.py
@@ -122,7 +122,7 @@
 
 
 def layer_kernel(
-    ng, nz,
+    ng,
     tok, mixg, gv, gg, taps, chg, mo, mlpg, up, dn,
     out,
     fgv, fgg, fmo, fup, fdn,
@@ -132,7 +132,8 @@
     ws, wr, lsem, tsem, nsem, ssem, rsem, fsem,
 ):
     f, t = lax.axis_index("fs"), lax.axis_index("tp")
-    p, z = lax.rem(f, ng), lax.div(f, ng)
+    x, y = lax.rem(f, 2), lax.rem(lax.div(f, 2), 2)
+    zp, zh = lax.rem(lax.div(f, 4), 2), lax.div(f, 8)
     sib = 1 - t
     L = tok.shape[0] // 2
     half = ng * L
@@ -142,11 +143,16 @@
     depth = gv.shape[0]
     sends = []
 
+    def flip(coord, bit):
+        return 1 - coord if bit else coord
+
     def chip(dq):
-        return lax.rem(p + dq, ng)
-
-    def plane(dz):
-        return lax.rem(z + dz, nz)
+        return flip(zp, dq // 2) * 2 + flip(x, dq % 2)
+
+    def fs_of(dq, do):
+        return flip(zh, do // 2) * 8 + flip(zp, dq // 2) * 4 + flip(y, do % 2) * 2 + flip(x, dq % 2)
+
+    p = chip(0)
 
     def push(src, dst, s_sem, r_sem, device):
         copy = pltpu.make_async_remote_copy(
@@ -163,8 +169,8 @@
         ).wait_recv()
 
     barrier = pltpu.get_barrier_semaphore()
-    peers = [(z * ng + chip(dq), u) for dq in range(1, ng) for u in (t, sib)]
-    peers += [(f, sib)] + [(plane(dz) * ng + p, t) for dz in range(1, nz)]
+    peers = [(fs_of(dq, 0), u) for dq in range(1, ng) for u in (t, sib)]
+    peers += [(f, sib), (fs_of(0, 1), t), (fs_of(0, 2), t)]
     for peer in peers:
         pl.semaphore_signal(barrier, inc=1, device_id=peer, device_id_type=MESH)
     pl.semaphore_wait(barrier, len(peers))
@@ -180,26 +186,33 @@
     def spread_in_plane(a):
         src, dst = weights[a]
         for dq in range(1, ng):
-            push(src(chip(dq)), dst(f), ws.at[a, dq], wr.at[a, ng - dq], (z * ng + chip(dq), t))
+            push(src(chip(dq)), dst(f), ws.at[a, dq], wr.at[a, dq], (fs_of(dq, 0), t))
 
     def spread_own(a):
         src, dst = weights[a]
-        for dz in range(1, nz):
-            push(src(p), dst(f), ws.at[a, dz * ng], wr.at[a, (nz - dz) * ng], (plane(dz) * ng + p, t))
+        for do in (2, 1):
+            push(src(p), dst(f), ws.at[a, do * ng], wr.at[a, do * ng], (fs_of(0, do), t))
 
     def forward(a):
         dst = weights[a][1]
         for dq in range(1, ng):
-            piece = dst(z * ng + chip(dq))
+            piece = dst(fs_of(dq, 0))
             arrived(piece, ws.at[a, 0], wr.at[a, dq])
-            for dz in range(1, nz):
-                push(piece, piece, ws.at[a, dz * ng + dq], wr.at[a, (nz - dz) * ng + dq], (plane(dz) * ng + p, t))
+            for do in (2, 1):
+                push(piece, piece, ws.at[a, do * ng + dq], wr.at[a, do * ng + dq], (fs_of(0, do), t))
+
+    def relay(a, which=(0, 1, 2, 3)):
+        dst = weights[a][1]
+        for dq in which:
+            piece = dst(fs_of(dq, 2))
+            arrived(piece, ws.at[a, 0], wr.at[a, 2 * ng + dq])
+            push(piece, piece, ws.at[a, 3 * ng + dq], wr.at[a, 3 * ng + dq], (fs_of(0, 1), t))
 
     def whole(a):
-        src, dst = weights[a]
-        for dz in range(1, nz):
+        dst = weights[a][1]
+        for do in (1, 3):
             for dq in range(ng):
-                arrived(dst(plane(dz) * ng + chip(dq)), ws.at[a, 0], wr.at[a, dz * ng + dq])
+                arrived(dst(fs_of(dq, do)), ws.at[a, 0], wr.at[a, do * ng + dq])
         local(a).wait()
 
     def local(a):
@@ -213,7 +226,7 @@
     for dq in range(1, ng):
         push(
             tok.at[rows_at(t * L, L)], tok_all.at[rows_at(t * half + p * L, L)],
-            tsem.at[0, dq], tsem.at[1, ng - dq], (z * ng + chip(dq), t),
+            tsem.at[0, dq], tsem.at[1, dq], (fs_of(dq, 0), t),
         )
     spread_in_plane(2)
     spread_own(2)
@@ -255,6 +268,8 @@
         arrived(tok_all.at[rows_at(start, L)], tsem.at[0, 0], tsem.at[3, dq])
         norm_rows(from_ref(tok_all, start), mixg, nrm, start)
 
+    relay(0)
+    relay(1)
     whole(0)
     whole(1)
     pad[...] = jnp.zeros_like(pad)
@@ -291,11 +306,12 @@
     slots = [(dq, du) for dq in range(ng) for du in range(2) if (dq, du) != (0, 0)]
     for dq, du in slots:
         push(
-            st, st_all.at[(ng - dq) % ng * 2 + du],
-            ssem.at[0, dq * 2 + du], ssem.at[1, (ng - dq) % ng * 2 + du],
-            (z * ng + chip(dq), t if du == 0 else sib),
+            st, st_all.at[dq * 2 + du],
+            ssem.at[0, dq * 2 + du], ssem.at[1, dq * 2 + du],
+            (fs_of(dq, 0), t if du == 0 else sib),
         )
     forward(3)
+    relay(2)
     for dq, du in slots:
         arrived(st_all.at[dq * 2 + du], ssem.at[0, 0], ssem.at[1, dq * 2 + du])
 
@@ -348,8 +364,8 @@
 
             lax.fori_loop(0, L // step, add, 0)
             push(
-                rdo.at[rows_at(base, L)], rdi.at[ng - dq - 1],
-                rsem.at[k, 2 * dq], rsem.at[k, 2 * (ng - dq) + 1], (z * ng + chip(dq), t),
+                rdo.at[rows_at(base, L)], rdi.at[dq - 1],
+                rsem.at[k, 2 * dq], rsem.at[k, 2 * dq + 1], (fs_of(dq, 0), t),
             )
 
     def reduced(sbi, rdi, i):
@@ -382,8 +398,9 @@
     lax.fori_loop(0, L // step, resid_rows, 0)
     mine = nm_all.at[rows_at(t * half + p * L, L)]
     for dq in range(1, ng):
-        push(mine, mine, nsem.at[0, dq], nsem.at[1, ng - dq], (z * ng + chip(dq), t))
+        push(mine, mine, nsem.at[0, dq], nsem.at[1, dq], (fs_of(dq, 0), t))
     push(mine, mine, nsem.at[2, 0], nsem.at[3, 0], (f, sib))
+    relay(3)
     for dq in range(1, ng):
         block = nm_all.at[rows_at(t * half + chip(dq) * L, L)]
         arrived(block, nsem.at[0, 0], nsem.at[1, dq])
@@ -404,9 +421,11 @@
         lax.fori_loop(0, hidden // 256, body, 0)
 
     up_half(t)
+    relay(4, (0, 1))
     for dq in range(ng):
         arrived(nm_all.at[rows_at(sib * half + chip(dq) * L, L)], nsem.at[0, 0], nsem.at[3, dq])
     up_half(sib)
+    relay(4, (2, 3))
     whole(4)
     reduce_rows(act, fdn, sbo2, sbi2, rdo2, rdi2, 1)
     wait_reduced(rdi2, 1)
@@ -460,7 +479,7 @@
         dma((2, blocks)), dma((2, 2 * ng)), dma((2,)),
     ]
     return pl.pallas_call(
-        functools.partial(layer_kernel, ng, nz),
+        functools.partial(layer_kernel, ng),
         out_shape=jax.ShapeDtypeStruct((rows, width), BF16),
         in_specs=[pl.BlockSpec(memory_space=vm)] * 10,
         out_specs=pl.BlockSpec(memory_space=vm),
@@ -480,8 +499,7 @@
     group = 4
     fits = (
         tp == 2
-        and fs % group == 0
-        and fs > group
+        and fs == group * 4
         and tokens.shape[0] == 2 * LEN
         and glu_value.shape[0] % 128 == 0
         and conv_taps.shape[1] % (group * 128) == 0

time: 293 us -> 262 us (0.89); the launches traced: 290 us -> 262 us
  Pallas kernels: 287 us -> 260 us
    pallas_call x1, Pallas kernels: 287 us -> 260 us  [fused_device(): pl.pallas_call(functools.partial(layer_kernel, ng), out_shape=jax.ShapeDt...]
where the time goes in v3:
time: 262 us
  Pallas kernels  260 us (99%)
    pallas_call x1, Pallas kernels, fused_device(): pl.pallas_call(functools.partial(layer_kernel, ng), out_shape=jax.ShapeDt...  260 us

profile of v3, /device:TPU:0, one launch (start us, length us, event | category | flops | bytes accessed | tf_op | source)
XLA Modules:
  0.0 262.1 jit_solution(1817957746869727924)
XLA Ops:
  0.0 259.8 %shard_map.100 = bf16[256,2048]{1,0:T(8,128)(2,1)} custom-call(bf16[256,2048]{1,0:T(8,128)(2,1)} %tok.1, f32[1,2048]{1,0:T(1,128)} %bitcast.3, bf16[128,1024]{1,0:T(8,128)(2,1)} %gv.1, bf16[128,1024]{1,0:T(8,128)(2,1)} %gg.1, f32[31,1024]{1,0:T(8,128)} %taps.1, f32[1,1024]{1,0:T(1,128)} %bitcast.5, bf16[1024,128]{1,0:T(8,128)(2,1)} %mo.1, ...), custom_call_target="tpu_custom_call" | custom-call | tf_op jit(solution)/shard_map/pallas_call | solution.py:481
  259.8 2.3 copy.12

commit v4 on v3

--- a/solution.py
+++ b/solution.py
@@ -221,15 +221,14 @@
 
     for a in (0, 1):
         spread_in_plane(a)
-    for a in (0, 1):
-        spread_own(a)
-    for dq in range(1, ng):
+    for dq in (2, 1):
         push(
             tok.at[rows_at(t * L, L)], tok_all.at[rows_at(t * half + p * L, L)],
             tsem.at[0, dq], tsem.at[1, dq], (fs_of(dq, 0), t),
         )
     spread_in_plane(2)
-    spread_own(2)
+    for a in (0, 1, 2):
+        spread_own(a)
     for a in (3, 4):
         spread_in_plane(a)
     for a in range(5):
@@ -255,9 +254,11 @@
         norm_rows(from_ref(tok, u * L), mixg, nrm, u * half + p * L)
     for a in (0, 1):
         forward(a)
-    for dq in range(1, ng):
+    for dq in (2, 1, 3):
         block = tok_all.at[rows_at(t * half + chip(dq) * L, L)]
         arrived(block, tsem.at[0, 0], tsem.at[1, dq])
+        if dq == 2:
+            push(block, block, tsem.at[0, 3], tsem.at[1, 3], (fs_of(1, 0), t))
         push(block, block, tsem.at[2, dq], tsem.at[3, dq], (f, sib))
         norm_rows(from_ref(tok_all, t * half + chip(dq) * L), mixg, nrm, t * half + chip(dq) * L)
     forward(2)
@@ -354,29 +355,35 @@
 
         lax.fori_loop(0, width // cols, mine, 0)
         arrived(sbi, rsem.at[k, 0], rsem.at[k, 1])
-        for dq in range(1, ng):
+        for dq in (3, 1, 2):
             base = chip(dq) * L
+            if dq == 2:
+                arrived(rdi.at[2], rsem.at[k, 0], rsem.at[k, 7])
 
             def add(i, _):
                 at = pl.ds(pl.multiple_of(base + i * step, step), step)
-                rdo[at, :] = (acc[at, :] + sbi[at, :].astype(F32)).astype(BF16)
+                value = acc[at, :] + sbi[at, :].astype(F32)
+                if dq == 2:
+                    value = value + rdi[2, pl.ds(pl.multiple_of(i * step, step), step), :].astype(F32)
+                rdo[at, :] = value.astype(BF16)
                 return 0
 
             lax.fori_loop(0, L // step, add, 0)
             push(
                 rdo.at[rows_at(base, L)], rdi.at[dq - 1],
-                rsem.at[k, 2 * dq], rsem.at[k, 2 * dq + 1], (fs_of(dq, 0), t),
+                rsem.at[k, 2 * dq], rsem.at[k, 2 * dq + 1],
+                (fs_of(2 if dq == 2 else 1, 0), t),
             )
 
     def reduced(sbi, rdi, i):
         at = pl.ds(pl.multiple_of(p * L + i * step, step), step)
         total = acc[at, :] + sbi[at, :].astype(F32)
-        for dq in range(1, ng):
+        for dq in (1, 2):
             total = total + rdi[dq - 1, pl.ds(pl.multiple_of(i * step, step), step), :].astype(F32)
         return total.astype(BF16).astype(F32)
 
     def wait_reduced(rdi, k):
-        for dq in range(1, ng):
+        for dq in (1, 2):
             arrived(rdi.at[dq - 1], rsem.at[k, 0], rsem.at[k, 2 * dq + 1])
 
     whole(2)
@@ -397,13 +404,16 @@
 
     lax.fori_loop(0, L // step, resid_rows, 0)
     mine = nm_all.at[rows_at(t * half + p * L, L)]
-    for dq in range(1, ng):
+    for dq in (2, 1):
         push(mine, mine, nsem.at[0, dq], nsem.at[1, dq], (fs_of(dq, 0), t))
     push(mine, mine, nsem.at[2, 0], nsem.at[3, 0], (f, sib))
-    relay(3)
-    for dq in range(1, ng):
+    for dq in (2, 1, 3):
         block = nm_all.at[rows_at(t * half + chip(dq) * L, L)]
+        if dq == 3:
+            relay(3)
         arrived(block, nsem.at[0, 0], nsem.at[1, dq])
+        if dq == 2:
+            push(block, block, nsem.at[0, 3], nsem.at[1, 3], (fs_of(1, 0), t))
         push(block, block, nsem.at[2, dq], nsem.at[3, dq], (f, sib))
 
     whole(3)

time: 262 us -> 274 us (1.046)
  Pallas kernels: 260 us -> 270 us
    pallas_call x1, Pallas kernels: 260 us -> 270 us  [fused_device(): pl.pallas_call(functools.partial(layer_kernel, ng), out_shape=jax.ShapeDt...]
where the time goes in v4:
time: 274 us; the launch traced here: 272 us
  Pallas kernels  270 us (99%)
    pallas_call x1, Pallas kernels, fused_device(): pl.pallas_call(functools.partial(layer_kernel, ng), out_shape=jax.ShapeDt...  270 us

profile of v4, /device:TPU:0, one launch (start us, length us, event | category | flops | bytes accessed | tf_op | source)
XLA Modules:
  0.0 272.1 jit_solution(9069925030276045748)
XLA Ops:
  0.0 269.8 %shard_map.100 = bf16[256,2048]{1,0:T(8,128)(2,1)} custom-call(bf16[256,2048]{1,0:T(8,128)(2,1)} %tok.1, f32[1,2048]{1,0:T(1,128)} %bitcast.3, bf16[128,1024]{1,0:T(8,128)(2,1)} %gv.1, bf16[128,1024]{1,0:T(8,128)(2,1)} %gg.1, f32[31,1024]{1,0:T(8,128)} %taps.1, f32[1,1024]{1,0:T(1,128)} %bitcast.5, bf16[1024,128]{1,0:T(8,128)(2,1)} %mo.1, ...), custom_call_target="tpu_custom_call" | custom-call | tf_op jit(solution)/shard_map/pallas_call | solution.py:491
  269.8 2.3 copy.12

commit v5 on v3

--- a/solution.py
+++ b/solution.py
@@ -312,6 +312,7 @@
         )
     forward(3)
     relay(2)
+    forward(4)
     for dq, du in slots:
         arrived(st_all.at[dq * 2 + du], ssem.at[0, 0], ssem.at[1, dq * 2 + du])
 
@@ -381,7 +382,6 @@
 
     whole(2)
     reduce_rows(hid, fmo, sbo1, sbi1, rdo1, rdi1, 0)
-    forward(4)
     wait_reduced(rdi1, 0)
 
     def resid_rows(i, _):

time: 262 us -> 252 us (0.962)
  Pallas kernels: 260 us -> 250 us
    pallas_call x1, Pallas kernels: 260 us -> 250 us  [fused_device(): pl.pallas_call(functools.partial(layer_kernel, ng), out_shape=jax.ShapeDt...]
where the time goes in v5:
time: 252 us
  Pallas kernels  250 us (99%)
    pallas_call x1, Pallas kernels, fused_device(): pl.pallas_call(functools.partial(layer_kernel, ng), out_shape=jax.ShapeDt...  250 us

profile of v5, /device:TPU:0, one launch (start us, length us, event | category | flops | bytes accessed | tf_op | source)
XLA Modules:
  0.0 252.2 jit_solution(17701521116738053665)
XLA Ops:
  0.0 249.9 %shard_map.100 = bf16[256,2048]{1,0:T(8,128)(2,1)} custom-call(bf16[256,2048]{1,0:T(8,128)(2,1)} %tok.1, f32[1,2048]{1,0:T(1,128)} %bitcast.3, bf16[128,1024]{1,0:T(8,128)(2,1)} %gv.1, bf16[128,1024]{1,0:T(8,128)(2,1)} %gg.1, f32[31,1024]{1,0:T(8,128)} %taps.1, f32[1,1024]{1,0:T(1,128)} %bitcast.5, bf16[1024,128]{1,0:T(8,128)(2,1)} %mo.1, ...), custom_call_target="tpu_custom_call" | custom-call | tf_op jit(solution)/shard_map/pallas_call | solution.py:481
  249.9 2.3 copy.12
